TPU v7x, 32 devices: a whole 2x2x4 slice. The times are simulated.
32 devices in a mesh: grp: 2 (over y), kv: 4 (over z), tp: 4 (over x, core).
Axes of the slice: x: 2, y: 2, z: 4, core: 2. Of those that a mesh axis runs over, the one named last changes fastest.
Arguments:
- tokens: bfloat16 [256, 4096], P('grp', 'kv'), parts along dimension 0, may hold values from -36 to 36
- span_lengths: int32 [256], P(('grp', 'kv')), parts along dimension 0, may hold values from 1 to 256, 13107 in all
- block_state: float32 [256, 64, 32, 64], P(('grp', 'kv'), 'tp'), parts along dimension 0, may hold values from -96 to 96
- key_cache: bfloat16 [256, 2048, 256], P(('grp', 'kv'), 'tp'), parts along dimension 0, may hold values from -6 to 6
- value_cache: bfloat16 [256, 4096, 256], P(('grp', 'kv'), 'tp'), parts along dimension 0, may hold values from -6 to 6
- decay_cache: float32 [256, 2048, 256], P(('grp', 'kv'), 'tp'), parts along dimension 0, may hold values from -34 to 0, as said below
- attn_gain: float32 [4096], P('kv'), may hold values from 0.1 to 1.9
- query_weight: bfloat16 [4096, 2048], P('kv', 'tp'), may hold values from -0.09375 to 0.09375
- key_weight: bfloat16 [4096, 2048], P('kv', 'tp'), may hold values from -0.09375 to 0.09375
- value_weight: bfloat16 [4096, 4096], P('kv', 'tp'), may hold values from -0.09375 to 0.09375
- gate_weight: bfloat16 [4096, 4096], P('kv', 'tp'), may hold values from -0.09375 to 0.09375
- decay_matrix: bfloat16 [4096, 2048], P('kv', 'tp'), may hold values from -0.09375 to 0.09375
- decay_offset_bias: float32 [2048], P('tp'), may hold values from -1.4 to 6
- head_gain: float32 [64], replicated, may hold values from 0.1 to 1.9
- out_weight: bfloat16 [4096, 4096], P('tp', 'kv'), may hold values from -0.09375 to 0.09375
- mixer_gain: float32 [4096], P('kv'), may hold values from 0.1 to 1.9
- up_weight: bfloat16 [4096, 16384], P('kv', 'tp'), may hold values from -0.09375 to 0.09375
- down_weight: bfloat16 [16384, 4096], P('tp', 'kv'), may hold values from -0.046875 to 0.046875
Outputs:
- layer_out: bfloat16 [256, 4096], P('grp', 'kv'), parts along dimension 0
There are 2 independent parts, one for each index of `grp`. A program takes and returns all parts, laid end to end along the dimension named above; an argument that names none is the same for every part. Nothing has to cross between parts.
Inputs may be any that keep to these rules, and one draw needn't show every extreme that they name: Cached positions at index span_lengths - 1 and beyond are unused. `decay_cache`: Non-increasing along positions.
All inputs are finite; a program needn't handle non-finite values. No bound on the sum of `span_lengths` on one device may be relied on, other than what follows from the above.
Results may differ from a plain program's by a relative error of at most 0.005.
The roundings to bfloat16 on the way count: a program that leaves them out, or rounds other values in their place, can miss the bound.
Values may be sent and summed in bfloat16 or wider, within the bound.
A program may use at most 128 MiB of HBM per device.

v0:
```python
import functools

import jax
import jax.numpy as jnp
from jax import lax
from jax.experimental import pallas as pl
from jax.experimental.pallas import tpu as pltpu
from jax.sharding import PartitionSpec as P

D = 4096
KEY_WIDTH = 32
DV = 64


NORM_EPS = 1e-06
DECAY_SOFTNESS = 16.0
MESH = pl.DeviceIdType.MESH
LANES = 128
F32 = jnp.float32
BF16 = jnp.bfloat16


def greet(axes):
    barrier = pltpu.get_barrier_semaphore()
    count = 0
    for axis in axes:
        size = lax.axis_size(axis)
        me = lax.axis_index(axis)
        for step in range(1, size):
            pl.semaphore_signal(
                barrier, inc=1, device_id={axis: lax.rem(me + step, size)}, device_id_type=MESH
            )
        count += size - 1
    pl.semaphore_wait(barrier, count)


def send(axis, step, src, dst, send_sem, recv_sem):
    size = lax.axis_size(axis)
    peer = lax.rem(lax.axis_index(axis) + step, size)
    copy = pltpu.make_async_remote_copy(
        src_ref=src(peer),
        dst_ref=dst,
        send_sem=send_sem,
        recv_sem=recv_sem,
        device_id={axis: peer},
        device_id_type=MESH,
    )
    copy.start()
    return copy


def project_kernel(
    parts, tok_ref, gain_ref, *refs
):
    weights, refs = refs[:5], refs[5:]
    sum_ref, sq_ref = refs[:2]
    wbuf, part, outgoing, incoming, sq_out, sq_in, wsem, ssem, rsem, qssem, qrsem = refs[2:]
    n, rows = outgoing.shape[0], outgoing.shape[1]
    me = lax.axis_index("kv")
    loads = []
    for i, (which, col, place, width) in enumerate(parts):
        load = pltpu.make_async_copy(
            weights[which].at[:, pl.ds(col, width)], wbuf.at[:, pl.ds(place, width)], wsem.at[i]
        )
        load.start()
        loads.append(load)
    x = tok_ref[...].astype(F32)
    scaled = (x * gain_ref[...]).astype(BF16)
    square = jnp.sum(x * x, axis=1, keepdims=True)
    sq_out[...] = jnp.broadcast_to(square, (x.shape[0], LANES)).reshape(sq_out.shape)
    greet(("kv",))
    copies = []
    for k in range(1, n):
        copies.append(
            send("kv", k, lambda p: sq_out.at[p], sq_in.at[k - 1], qssem.at[k - 1], qrsem.at[k - 1])
        )
    for i, (which, col, place, width) in enumerate(parts):
        loads[i].wait()
        cols = pl.ds(place, width)
        got = jnp.dot(scaled, wbuf[:, cols], preferred_element_type=F32).reshape(n, rows, width)
        part[:, :, cols] = got
        outgoing[:, :, cols] = got.astype(BF16)
        for k in SEND_ORDER(n):
            copies.append(
                send(
                    "kv",
                    k,
                    lambda p: outgoing.at[p, :, cols],
                    incoming.at[k - 1, :, cols],
                    ssem.at[k - 1, i],
                    rsem.at[k - 1, i],
                )
            )
    for copy in copies:
        copy.wait_recv()
    total = part[me]
    square = sq_out[me]
    for k in range(n - 1):
        total = total + incoming[k].astype(F32)
        square = square + sq_in[k]
    sum_ref[...] = total
    sq_ref[...] = square
    for copy in copies:
        copy.wait_send()


def SEND_ORDER(n):
    return sorted(range(1, n), key=lambda k: -min(k, n - k))


def project(tokens, gain, weights):
    n = lax.axis_size("kv")
    rows = tokens.shape[0] // n
    parts, place = [], 0
    for which, w in enumerate(weights):
        width = min(512, w.shape[1])
        for col in range(0, w.shape[1], width):
            parts.append((which, col, place, width))
            place += width
    vmem = pl.BlockSpec(memory_space=pltpu.VMEM)
    return pl.pallas_call(
        functools.partial(project_kernel, parts),
        out_shape=(
            jax.ShapeDtypeStruct((rows, place), F32),
            jax.ShapeDtypeStruct((rows, LANES), F32),
        ),
        in_specs=[vmem, vmem] + [pl.BlockSpec(memory_space=pltpu.HBM)] * 5,
        out_specs=(vmem, vmem),
        scratch_shapes=[
            pltpu.VMEM((tokens.shape[1], place), BF16),
            pltpu.VMEM((n, rows, place), F32),
            pltpu.VMEM((n, rows, place), BF16),
            pltpu.VMEM((n - 1, rows, place), BF16),
            pltpu.VMEM((n, rows, LANES), F32),
            pltpu.VMEM((n - 1, rows, LANES), F32),
            pltpu.SemaphoreType.DMA((len(parts),)),
            pltpu.SemaphoreType.DMA((n - 1, len(parts))),
            pltpu.SemaphoreType.DMA((n - 1, len(parts))),
            pltpu.SemaphoreType.DMA((n - 1,)),
            pltpu.SemaphoreType.DMA((n - 1,)),
        ],
        compiler_params=pltpu.CompilerParams(
            collective_id=0, has_side_effects=True, vmem_limit_bytes=62 << 20
        ),
        name="project",
    )(tokens, gain.reshape(1, -1), *weights)


NT = (((1,), (1,)), ((), ()))


def attend_kernel(
    len_ref, last_ref, sum_ref, sq_ref, bias_ref, hg_ref, k1, k2a, k2b, d1, d2a, d2b,
    v1, v2a, v2b, st, out_ref, q_t, ld_t, qk_t, vn, gs, now_s, q_s, hist, raw,
):
    step = pl.program_id(0)
    rows = out_ref.shape[0]
    heads = st.shape[1]
    keys, vals = heads * KEY_WIDTH, heads * DV
    lane = lax.broadcasted_iota(jnp.int32, (1, LANES), 1)

    @pl.when(step == 0)
    def _():
        scale = lax.rsqrt(sq_ref[:, :1] / D + NORM_EPS)
        q = sum_ref[:, :keys] * scale * KEY_WIDTH ** (-0.5)
        key_new = sum_ref[:, keys : 2 * keys] * scale
        at = 2 * keys
        vn[...] = sum_ref[:, at : at + vals] * scale
        g = sum_ref[:, at + vals : at + 2 * vals] * scale
        gs[...] = g * (1.0 / (1.0 + jnp.exp(-g))) * jnp.concatenate([hg_ref[...]] * heads, axis=1)
        x = sum_ref[:, at + 2 * vals :] * scale + bias_ref[...]
        ld = (jnp.minimum(x, 0.0) - jnp.log1p(jnp.exp(-jnp.abs(x)))) / DECAY_SOFTNESS
        spare = jnp.zeros((LANES - rows, keys), F32)
        q_t[...] = jnp.concatenate([q, spare], axis=0).T
        ld_t[...] = jnp.concatenate([ld, spare], axis=0).T
        pick = lax.broadcasted_iota(jnp.int32, (heads, keys), 1) // KEY_WIDTH
        pick = (pick == lax.broadcasted_iota(jnp.int32, (heads, keys), 0)).astype(F32)
        qk_t[...] = lax.dot_general(
            pick,
            jnp.concatenate([q * key_new, spare], axis=0),
            NT,
            precision=lax.Precision.HIGHEST,
            preferred_element_type=F32,
        )

    seconds = ((k2a, d2a, v2a), (k2b, d2b, v2b))
    lengths = [len_ref[2 * step + j] for j in range(2)]
    mine = [lane == 2 * step + j for j in range(2)]
    wide = (keys, LANES)

    def block(j, k, d, v, offset):
        s = k.astype(F32) * q_s[j] * jnp.exp(now_s[j] - d)
        s = jnp.sum(s.reshape(heads, KEY_WIDTH, LANES), axis=1)
        s = jnp.where(lane + offset < lengths[j] - 1, s, 0.0).astype(BF16)
        return lax.dot_general(s, v, NT, preferred_element_type=F32)

    for j in range(2):
        prev = jnp.where(lane == lengths[j] - 2, d1[j], 0.0)
        prev = prev + jnp.where(lane + LANES == lengths[j] - 2, seconds[j][1][0], 0.0)
        own_decay = jnp.where(mine[j], ld_t[...], 0.0)
        now_s[j] = jnp.broadcast_to(jnp.sum(prev + own_decay, axis=1, keepdims=True), wide)
        q = jnp.sum(jnp.where(mine[j], q_t[...], 0.0), axis=1, keepdims=True)
        q_s[j] = jnp.broadcast_to(q, wide)
    for j in range(2):
        hist[j] = block(j, k1[j], d1[j], v1[j], 0)
    for j in range(2):

        @pl.when(lengths[j] - 1 > LANES)
        def _(j=j):
            k2, d2, v2 = seconds[j]
            hist[j] += block(j, k2[0], d2[0], v2[0], LANES)

    own = lax.broadcasted_iota(jnp.int32, (heads, vals), 1) // DV
    own = own == lax.broadcasted_iota(jnp.int32, (heads, vals), 0)
    for j in range(2):
        weight = (q_s[j] * jnp.exp(now_s[j]))[:, :DV]
        carried = weight * st[j].reshape(keys, DV)
        carried = jnp.sum(carried.reshape(heads, KEY_WIDTH, DV), axis=1)
        carried = jnp.concatenate([carried] * heads, axis=1)
        qk = jnp.sum(jnp.where(mine[j], qk_t[...], 0.0), axis=1, keepdims=True)
        row = pl.ds(2 * step + j, 1)
        whole = hist[j] + carried + qk * vn[row, :]
        whole = jnp.where(own, whole, 0.0)
        mean = jnp.sum(whole * whole, axis=1, keepdims=True) / DV
        whole = whole * lax.rsqrt(mean + NORM_EPS)
        raw[row, :] = jnp.sum(whole, axis=0, keepdims=True)

    @pl.when(step == pl.num_programs(0) - 1)
    def _():
        out_ref[...] = (raw[...] * gs[...]).astype(BF16)


def attend(span_lengths, sums, square, bias, head_gain, keys, values, decays, state):
    rows, heads = state.shape[:2]
    kw, vw = heads * KEY_WIDTH, heads * DV
    order = jnp.arange(rows, dtype=jnp.int32)
    needed = jnp.where(span_lengths - 1 > LANES, order, order % 2)
    before = (order[None, :] <= order[:, None]) & (order[None, :] % 2 == order[:, None] % 2)
    last = jnp.max(jnp.where(before, needed[None, :], 0), axis=1)

    def first(width):
        return pl.BlockSpec((2, width, LANES), lambda i, ln, la: (i, 0, 0))

    def second(width, j):
        return pl.BlockSpec((1, width, LANES), lambda i, ln, la: (la[2 * i + j], 0, 1))

    def fixed(shape):
        return pl.BlockSpec(shape, lambda i, ln, la: (0,) * len(shape))

    return pl.pallas_call(
        attend_kernel,
        out_shape=jax.ShapeDtypeStruct((rows, vw), BF16),
        grid_spec=pltpu.PrefetchScalarGridSpec(
            num_scalar_prefetch=2,
            grid=(rows // 2,),
            in_specs=[
                fixed(sums.shape),
                fixed(square.shape),
                fixed((1, kw)),
                fixed((1, DV)),
                first(kw),
                second(kw, 0),
                second(kw, 1),
                first(kw),
                second(kw, 0),
                second(kw, 1),
                first(vw),
                second(vw, 0),
                second(vw, 1),
                pl.BlockSpec((2, heads, KEY_WIDTH, DV), lambda i, ln, la: (i, 0, 0, 0)),
            ],
            out_specs=fixed((rows, vw)),
            scratch_shapes=[
                pltpu.VMEM((kw, LANES), F32),
                pltpu.VMEM((kw, LANES), F32),
                pltpu.VMEM((heads, LANES), F32),
                pltpu.VMEM((rows, vw), F32),
                pltpu.VMEM((rows, vw), F32),
                pltpu.VMEM((2, kw, LANES), F32),
                pltpu.VMEM((2, kw, LANES), F32),
                pltpu.VMEM((2, heads, vw), F32),
                pltpu.VMEM((rows, vw), F32),
            ],
        ),
        compiler_params=pltpu.CompilerParams(
            dimension_semantics=("arbitrary",), vmem_limit_bytes=62 << 20
        ),
        name="attend",
    )(
        span_lengths, last, sums, square, bias.reshape(1, -1), head_gain.reshape(1, -1),
        keys, keys, keys, decays, decays, decays, values, values, values, state,
    )


def finish_kernel(
    mixed_ref, tok_ref, gain_ref, ow_ref, uw_ref, dw_ref, out_ref,
    ow, uw, dw, gath, part, t_out, t_in, resid, scaled, sq_out, sq_in,
    u_part, u_own, u_out, u_in, hid, total, t_out2, t_in2, done,
    wsem, g_s, g_r, a_s, a_r, b_s, b_r, q_s, q_r, u_s, u_r, h_s, h_r, c_s, c_r, e_s, e_r,
):
    n, m = lax.axis_size("kv"), lax.axis_size("tp")
    me, col = lax.axis_index("kv"), lax.axis_index("tp")
    chunks = u_s.shape[1]
    width = u_out.shape[2] // chunks
    loads = [
        pltpu.make_async_copy(ow_ref, ow, wsem.at[0]),
    ]
    for c in range(chunks):
        at = pl.ds(c * width, width)
        loads.append(pltpu.make_async_copy(uw_ref.at[:, at], uw.at[:, at], wsem.at[1 + c]))
    loads.append(pltpu.make_async_copy(dw_ref, dw, wsem.at[1 + chunks]))
    for load in loads:
        load.start()
    greet(("kv", "tp"))
    copies = []

    def wait_all(group):
        for copy in group:
            copy.wait_recv()
        copies.extend(group)

    group = [
        send("kv", k, lambda p: mixed_ref, gath.at[me], g_s.at[k - 1], g_r.at[k - 1])
        for k in SEND_ORDER(n)
    ]
    gath[me] = mixed_ref[...]
    wait_all(group)
    loads[0].wait()
    rows = gath.shape[0] * gath.shape[1]

    def over_tp(value, outgoing, incoming, ss, rs):
        part[...] = value.reshape(part.shape)
        outgoing[...] = value.reshape(part.shape).astype(BF16)
        group = [
            send("tp", k, lambda p: outgoing.at[p], incoming.at[k - 1], ss.at[k - 1], rs.at[k - 1])
            for k in range(1, m)
        ]
        wait_all(group)
        result = part[col]
        for k in range(m - 1):
            result = result + incoming[k].astype(F32)
        return result

    def to_tp(buffer, ss, rs):
        group = [
            send("tp", k, lambda p: buffer.at[col], buffer.at[col], ss.at[k - 1], rs.at[k - 1])
            for k in range(1, m)
        ]
        wait_all(group)

    x = gath[...].reshape(rows, gath.shape[2])
    attn = over_tp(jnp.dot(x, ow[...], preferred_element_type=F32), t_out, t_in, a_s, a_r)
    resid[col] = (tok_ref[col].astype(F32) + attn).astype(BF16)
    to_tp(resid, b_s, b_r)
    whole = resid[...].reshape(rows, resid.shape[2]).astype(F32)
    square = jnp.sum(whole * whole, axis=1, keepdims=True)
    sq_out[...] = jnp.broadcast_to(square, (rows, LANES)).reshape(sq_out.shape)
    sq_group = [
        send("kv", k, lambda p: sq_out.at[p], sq_in.at[k - 1], q_s.at[k - 1], q_r.at[k - 1])
        for k in SEND_ORDER(n)
    ]
    scaled[...] = (whole * gain_ref[...]).astype(BF16)

    def toward(bit, ref, ss, rs):
        peer = me + bit - 2 * bit * (me // bit % 2)
        copy = pltpu.make_async_remote_copy(
            src_ref=ref(peer), dst_ref=ref(peer), send_sem=ss, recv_sem=rs,
            device_id={"kv": peer}, device_id_type=MESH,
        )
        copy.start()
        return copy

    groups = []
    for c in range(chunks):
        at = pl.ds(c * width, width)
        loads[1 + c].wait()
        got = jnp.dot(scaled[...], uw[:, at], preferred_element_type=F32)
        got = got.reshape(u_part.shape)
        u_part[...] = got
        u_out[:, :, at] = got.astype(BF16)
        groups.append(
            [
                send(
                    "kv", k, lambda p: u_out.at[p, :, at], u_in.at[k - 1, :, at],
                    u_s.at[k - 1, c], u_r.at[k - 1, c],
                )
                for k in SEND_ORDER(n)
            ]
        )
        u_own[:, at] = u_part[me]
    wait_all(sq_group)
    square = sq_out[me]
    for k in range(n - 1):
        square = square + sq_in[k]
    scale = lax.rsqrt(square[:, :1] / D + NORM_EPS)
    hidden_groups = []
    for c in range(chunks):
        at = pl.ds(c * width, width)
        wait_all(groups[c])
        got = u_own[:, at]
        for k in range(n - 1):
            got = got + u_in[k, :, at].astype(F32)
        hid[me, :, at] = jnp.square(jnp.maximum(got * scale, 0.0)).astype(BF16)
        hidden_groups.append(
            [
                toward(2, lambda p: hid.at[me, :, at], h_s.at[0, c], h_r.at[0, c]),
                toward(1, lambda p: hid.at[me, :, at], h_s.at[1, c], h_r.at[1, c]),
            ]
        )
    for c in range(chunks):
        at = pl.ds(c * width, width)
        wait_all(hidden_groups[c][:1])
        far = me + 2 - 4 * (me // 2)
        hidden_groups[c].append(
            toward(1, lambda p: hid.at[far, :, at], h_s.at[2, c], h_r.at[2, c])
        )
    loads[1 + chunks].wait()
    for c in range(chunks):
        at = pl.ds(c * width, width)
        wait_all(hidden_groups[c][1:])
        got = jnp.dot(
            hid[:, :, at].reshape(rows, width), dw[at, :], preferred_element_type=F32
        )
        if c == 0:
            total[...] = got
        else:
            total[...] += got
    mixer = over_tp(total[...], t_out2, t_in2, c_s, c_r)
    done[col] = (resid[col].astype(F32) + mixer).astype(BF16)
    to_tp(done, e_s, e_r)
    out_ref[...] = done[...]
    for copy in copies:
        copy.wait_send()


def finish(mixed, tokens, gain, out_weight, up_weight, down_weight):
    n, m = lax.axis_size("kv"), lax.axis_size("tp")
    rows, feats = tokens.shape
    vals, hidden = out_weight.shape[0], up_weight.shape[1]
    own, share = rows // n, rows // m
    chunks = 4
    vmem = pl.BlockSpec(memory_space=pltpu.VMEM)
    hbm = pl.BlockSpec(memory_space=pltpu.HBM)
    dma = pltpu.SemaphoreType.DMA
    out = pl.pallas_call(
        finish_kernel,
        out_shape=jax.ShapeDtypeStruct((m, share, feats), BF16),
        in_specs=[vmem, vmem, vmem, hbm, hbm, hbm],
        out_specs=vmem,
        scratch_shapes=[
            pltpu.VMEM(out_weight.shape, BF16),
            pltpu.VMEM(up_weight.shape, BF16),
            pltpu.VMEM(down_weight.shape, BF16),
            pltpu.VMEM((n, own, vals), BF16),
            pltpu.VMEM((m, share, feats), F32),
            pltpu.VMEM((m, share, feats), BF16),
            pltpu.VMEM((m - 1, share, feats), BF16),
            pltpu.VMEM((m, share, feats), BF16),
            pltpu.VMEM((rows, feats), BF16),
            pltpu.VMEM((n, own, LANES), F32),
            pltpu.VMEM((n - 1, own, LANES), F32),
            pltpu.VMEM((n, own, hidden // chunks), F32),
            pltpu.VMEM((own, hidden), F32),
            pltpu.VMEM((n, own, hidden), BF16),
            pltpu.VMEM((n - 1, own, hidden), BF16),
            pltpu.VMEM((n, own, hidden), BF16),
            pltpu.VMEM((rows, feats), F32),
            pltpu.VMEM((m, share, feats), BF16),
            pltpu.VMEM((m - 1, share, feats), BF16),
            pltpu.VMEM((m, share, feats), BF16),
            dma((2 + chunks,)),
            dma((n - 1,)),
            dma((n - 1,)),
            dma((m - 1,)),
            dma((m - 1,)),
            dma((m - 1,)),
            dma((m - 1,)),
            dma((n - 1,)),
            dma((n - 1,)),
            dma((n - 1, chunks)),
            dma((n - 1, chunks)),
            dma((n - 1, chunks)),
            dma((n - 1, chunks)),
            dma((m - 1,)),
            dma((m - 1,)),
            dma((m - 1,)),
            dma((m - 1,)),
        ],
        compiler_params=pltpu.CompilerParams(
            collective_id=1, has_side_effects=True, vmem_limit_bytes=62 << 20
        ),
        name="finish",
    )(
        mixed, tokens.reshape(m, share, feats), gain.reshape(1, -1),
        out_weight, up_weight, down_weight,
    )
    return out.reshape(rows, feats)


def kernel_shards(
    tokens,
    span_lengths,
    block_state,
    key_cache,
    value_cache,
    decay_cache,
    attn_gain,
    query_weight,
    key_weight,
    value_weight,
    gate_weight,
    decay_matrix,
    decay_offset_bias,
    head_gain,
    out_weight,
    mixer_gain,
    up_weight,
    down_weight,
):
    weights = (query_weight, key_weight, value_weight, gate_weight, decay_matrix)
    sums, square = project(tokens, attn_gain, weights)
    mixed = attend(
        span_lengths, sums, square, decay_offset_bias, head_gain,
        key_cache, value_cache, decay_cache, block_state,
    )
    return finish(mixed, tokens, mixer_gain, out_weight, up_weight, down_weight)


def fits(tokens, block_state, key_cache):
    rows, heads = block_state.shape[:2]
    share = tokens.shape[0] // lax.axis_size("tp")
    return (
        lax.axis_size("kv") == 4
        and rows % 16 == 0
        and share % 16 == 0
        and heads % 8 == 0
        and rows < LANES
        and key_cache.shape[2] == 2 * LANES
    )


def shards(
    tokens,
    span_lengths,
    block_state,
    key_cache,
    value_cache,
    decay_cache,
    attn_gain,
    query_weight,
    key_weight,
    value_weight,
    gate_weight,
    decay_matrix,
    decay_offset_bias,
    head_gain,
    out_weight,
    mixer_gain,
    up_weight,
    down_weight,
):
    if fits(tokens, block_state, key_cache):
        return kernel_shards(
            tokens, span_lengths, block_state, key_cache, value_cache, decay_cache,
            attn_gain, query_weight, key_weight, value_weight, gate_weight, decay_matrix,
            decay_offset_bias, head_gain, out_weight, mixer_gain, up_weight, down_weight,
        )
    seq_count = block_state.shape[0]
    head_count = block_state.shape[1]
    span_size = key_cache.shape[2]
    whole_rows = tokens.astype(jnp.float32)
    square_sum = jnp.sum(whole_rows * whole_rows, axis=1)
    scaled = (whole_rows * attn_gain).astype(jnp.bfloat16)
    query_part = jnp.dot(scaled, query_weight, preferred_element_type=jnp.float32)
    key_part = jnp.dot(scaled, key_weight, preferred_element_type=jnp.float32)
    value_part = jnp.dot(scaled, value_weight, preferred_element_type=jnp.float32)
    gate_part = jnp.dot(scaled, gate_weight, preferred_element_type=jnp.float32)
    decay_part = jnp.dot(scaled, decay_matrix, preferred_element_type=jnp.float32)
    square_total = lax.psum(square_sum, "kv")
    query_sum, key_sum, value_sum, gate_sum, decay_running_sum = (
        lax.psum_scatter(query_part, "kv", scatter_dimension=0, tiled=True),
        lax.psum_scatter(key_part, "kv", scatter_dimension=0, tiled=True),
        lax.psum_scatter(value_part, "kv", scatter_dimension=0, tiled=True),
        lax.psum_scatter(gate_part, "kv", scatter_dimension=0, tiled=True),
        lax.psum_scatter(decay_part, "kv", scatter_dimension=0, tiled=True),
    )
    own_square = lax.dynamic_slice_in_dim(square_total, lax.axis_index("kv") * seq_count, seq_count)
    scale_per_row = lax.rsqrt(own_square / D + NORM_EPS)[:, None]
    query = (query_sum * scale_per_row * KEY_WIDTH ** (-0.5)).reshape(
        seq_count, head_count, KEY_WIDTH
    )
    key_new = (key_sum * scale_per_row).reshape(seq_count, head_count, KEY_WIDTH)
    value_new = (value_sum * scale_per_row).reshape(seq_count, head_count, DV)
    gate = gate_sum * scale_per_row
    logarithm_decay = (
        jax.nn.log_sigmoid(decay_running_sum * scale_per_row + decay_offset_bias) / DECAY_SOFTNESS
    )
    token_place = lax.broadcasted_iota(jnp.int32, (1, 1, span_size), 2)
    lengths_now = span_lengths[:, None, None]
    previous = jnp.sum(jnp.where(token_place == lengths_now - 2, decay_cache, 0.0), axis=-1)
    now_decay = (previous + logarithm_decay).reshape(seq_count, head_count, KEY_WIDTH)
    decays_span = decay_cache.reshape(seq_count, head_count, KEY_WIDTH, span_size)
    in_use = (token_place < lengths_now - 1)[:, :, None, :]
    factor = jnp.where(in_use, jnp.exp(now_decay[..., None] - decays_span), 0.0)
    keys_span = key_cache.reshape(seq_count, head_count, KEY_WIDTH, span_size)
    scores = jnp.sum(query[..., None] * keys_span.astype(jnp.float32) * factor, axis=2)
    scores_low = scores.astype(jnp.bfloat16)
    values_span = value_cache.reshape(seq_count, head_count, DV, span_size)
    history = jnp.einsum(
        "nhs,nhvs->nhv", scores_low, values_span, preferred_element_type=jnp.float32
    )
    carried = jnp.einsum(
        "nhc,nhcv->nhv", query * jnp.exp(now_decay), block_state, precision=lax.Precision.HIGHEST
    )
    own_term = jnp.sum(query * key_new, axis=-1, keepdims=True) * value_new
    raw = carried + history + own_term
    normed = raw * lax.rsqrt(jnp.mean(raw * raw, axis=-1, keepdims=True) + NORM_EPS) * head_gain
    mixed = (normed.reshape(seq_count, head_count * DV) * jax.nn.silu(gate)).astype(jnp.bfloat16)
    attn_terms = jnp.dot(
        lax.all_gather(mixed, "kv", axis=0, tiled=True),
        out_weight,
        preferred_element_type=jnp.float32,
    )
    attn_out = lax.psum(attn_terms, "tp")
    resid = (whole_rows + attn_out).astype(jnp.bfloat16)
    resid_rows = resid.astype(jnp.float32)
    mixer_square = jnp.sum(resid_rows * resid_rows, axis=1)
    mixer_scaled = (resid_rows * mixer_gain).astype(jnp.bfloat16)
    up_part = jnp.dot(mixer_scaled, up_weight, preferred_element_type=jnp.float32)
    up_share, square_share = (
        lax.psum_scatter(up_part, "kv", scatter_dimension=0, tiled=True),
        lax.psum_scatter(mixer_square, "kv", scatter_dimension=0, tiled=True),
    )
    hidden_share = jnp.square(
        jax.nn.relu(up_share * lax.rsqrt(square_share / D + NORM_EPS)[:, None])
    )
    hidden_share = hidden_share.astype(jnp.bfloat16)
    down_terms = jnp.dot(
        lax.all_gather(hidden_share, "kv", axis=0, tiled=True),
        down_weight,
        preferred_element_type=jnp.float32,
    )
    mixer_out = lax.psum(down_terms, "tp")
    return (resid_rows + mixer_out).astype(jnp.bfloat16)


def solution(mesh):
    placed = (
        P("grp", "kv"),
        P(("grp", "kv")),
        P(("grp", "kv"), "tp", None, None),
        P(("grp", "kv"), "tp", None),
        P(("grp", "kv"), "tp", None),
        P(("grp", "kv"), "tp", None),
        P("kv"),
        P("kv", "tp"),
        P("kv", "tp"),
        P("kv", "tp"),
        P("kv", "tp"),
        P("kv", "tp"),
        P("tp"),
        P(),
        P("tp", "kv"),
        P("kv"),
        P("kv", "tp"),
        P("tp", "kv"),
    )
    return jax.shard_map(
        shards, mesh=mesh, in_specs=placed, out_specs=P("grp", "kv"), check_vma=False
    )
```

profile of v0, /device:TPU:1, one launch (start us, length us, event | category | flops | bytes accessed | tf_op | source)
XLA Modules:
  0.0 129.4 jit_solution(13409519112639355076)
XLA Ops:
  0.0 0.7 compare_select_fusion
  0.7 0.8 select_reduce_fusion.last_ref
  1.4 27.5 %project.1 = (f32[32,3584]{1,0:T(8,128)}, f32[32,128]{1,0:T(8,128)}) custom-call(bf16[128,1024]{1,0:T(8,128)(2,1)} %tok_ref.1, f32[1,1024]{1,0:T(1,128)} %bitcast.8, bf16[1024,512]{1,0:T(8,128)(2,1)} %refs_0_.1, bf16[1024,512]{1,0:T(8,128)(2,1)} %refs_1_.1, bf16[1024,1024]{1,0:T(8,128)(2,1)} %refs_2_.1, bf16[1024,1024]{1,0:T(8,128)(2,1)} %refs_3_.1, ...), custom_call_target="tpu_custom_call" | custom-call | tf_op jit(solution)/shard_map/project/pallas_call | solution.py:121
  29.0 25.5 %attend.1.mixed_ref = bf16[32,1024]{1,0:T(8,128)(2,1)} custom-call(s32[32]{0:T(128)} %len_ref.1, s32[32]{0:T(128)} %select_reduce_fusion.last_ref, f32[32,3584]{1,0:T(8,128)} %get-tuple-element.7.sum_ref, f32[32,128]{1,0:T(8,128)} %get-tuple-element.8.sq_ref, f32[1,512]{1,0:T(1,128)} %bitcast.10, f32[1,64]{1,0:T(1,128)} %bitcast.11, ...), custom_call_target="tpu_custom_call" | custom-call | tf_op jit(solution)/shard_map/attend/pallas_call | solution.py:250
  54.4 73.2 %finish.1 = bf16[4,32,1024]{2,1,0:T(8,128)(2,1)} custom-call(bf16[32,1024]{1,0:T(8,128)(2,1)} %attend.1.mixed_ref, bf16[4,32,1024]{2,1,0:T(8,128)(2,1)} %bitcast.6, f32[1,1024]{1,0:T(1,128)} %bitcast.9, bf16[1024,1024]{1,0:T(8,128)(2,1)} %ow_ref.1, bf16[1024,4096]{1,0:T(8,128)(2,1)} %uw_ref.1, bf16[4096,1024]{1,0:T(8,128)(2,1)} %dw_ref.1), custom_call_target="tpu_custom_call" | custom-call | tf_op jit(solution)/shard_map/finish/pallas_call | solution.py:445
  127.7 1.7 %copy.20 = bf16[128,1024]{1,0:T(8,128)(2,1)} copy(bf16[128,1024]{1,0:T(8,128)(2,1)} %bitcast.7) | data formatting | bytes 524288
where the time goes:
time: 131 us; the launch traced here: 129 us
  Pallas kernels  126 us (96%)
  local copies, waits for them, and re-layouts  1.67 us (1%)
  other arithmetic  1.43 us (1%)
    pallas_call x1, Pallas kernels, finish(): pl.pallas_call(finish_kernel, out_shape=jax.ShapeDtypeStruct((m, share, f...  73.2 us
    pallas_call x1, Pallas kernels, project(): pl.pallas_call(functools.partial(project_kernel, parts), out_shape=(jax.S...  27.5 us
    pallas_call x1, Pallas kernels, attend(): pl.pallas_call(attend_kernel, out_shape=jax.ShapeDtypeStruct((rows, vw),...  25.5 us

commit v1 on v0

--- a/solution.py
+++ b/solution.py
@@ -49,14 +49,51 @@
     return copy
 
 
-def project_kernel(
-    parts, tok_ref, gain_ref, *refs
+def SEND_ORDER(n):
+    return sorted(range(1, n), key=lambda k: -min(k, n - k))
+
+
+NT = (((1,), (1,)), ((), ()))
+LOG2E = 1.4426950408889634
+
+
+def split3(x):
+    high = x.astype(BF16).astype(F32)
+    rest = x - high
+    mid = rest.astype(BF16).astype(F32)
+    return high, mid, rest - mid
+
+
+def stack2(y):
+    high = y.astype(BF16)
+    low = (y - high.astype(F32)).astype(BF16)
+    return jnp.concatenate([high, low], axis=0)
+
+
+def attend_kernel(
+    parts, slots, len_ref, tok_ref, gain_ref, bias_ref, hg_ref, *refs
 ):
     weights, refs = refs[:5], refs[5:]
-    sum_ref, sq_ref = refs[:2]
-    wbuf, part, outgoing, incoming, sq_out, sq_in, wsem, ssem, rsem, qssem, qrsem = refs[2:]
+    k_ref, v_ref, d_ref, st_ref, out_ref = refs[:5]
+    (
+        wbuf, part, outgoing, incoming, sq_out, sq_in, kbuf, vbuf, dbuf, sbuf,
+        q_t, ld_t, prev_t, a3, ab, score, carry, raw, mixed, gath,
+        wsem, csem, ssem, rsem, qssem, qrsem, g_s, g_r,
+    ) = refs[5:]
     n, rows = outgoing.shape[0], outgoing.shape[1]
+    heads = st_ref.shape[1]
+    keys, vals, span = heads * KEY_WIDTH, heads * DV, k_ref.shape[2]
+    sub = keys // KEY_WIDTH * 8
     me = lax.axis_index("kv")
+
+    def fetch(j, slot):
+        for i, (src, dst) in enumerate(((d_ref, dbuf), (k_ref, kbuf), (v_ref, vbuf), (st_ref, sbuf))):
+            pltpu.make_async_copy(src.at[j], dst.at[slot], csem.at[i, slot]).start()
+
+    def arrived(which, slot):
+        src, dst = ((d_ref, dbuf), (k_ref, kbuf), (v_ref, vbuf), (st_ref, sbuf))[which]
+        pltpu.make_async_copy(src.at[0], dst.at[slot], csem.at[which, slot]).wait()
+
     loads = []
     for i, (which, col, place, width) in enumerate(parts):
         load = pltpu.make_async_copy(
@@ -64,6 +101,11 @@
         )
         load.start()
         loads.append(load)
+
+    @pl.loop(0, slots)
+    def _(j):
+        fetch(j, j)
+
     x = tok_ref[...].astype(F32)
     scaled = (x * gain_ref[...]).astype(BF16)
     square = jnp.sum(x * x, axis=1, keepdims=True)
@@ -74,58 +116,196 @@
         copies.append(
             send("kv", k, lambda p: sq_out.at[p], sq_in.at[k - 1], qssem.at[k - 1], qrsem.at[k - 1])
         )
+    groups = []
     for i, (which, col, place, width) in enumerate(parts):
         loads[i].wait()
         cols = pl.ds(place, width)
         got = jnp.dot(scaled, wbuf[:, cols], preferred_element_type=F32).reshape(n, rows, width)
         part[:, :, cols] = got
         outgoing[:, :, cols] = got.astype(BF16)
-        for k in SEND_ORDER(n):
-            copies.append(
-                send(
-                    "kv",
-                    k,
-                    lambda p: outgoing.at[p, :, cols],
-                    incoming.at[k - 1, :, cols],
-                    ssem.at[k - 1, i],
-                    rsem.at[k - 1, i],
-                )
+        groups.append([
+            send(
+                "kv", k, lambda p: outgoing.at[p, :, cols], incoming.at[k - 1, :, cols],
+                ssem.at[k - 1, i], rsem.at[k - 1, i],
             )
+            for k in SEND_ORDER(n)
+        ])
+
+    lane = lax.broadcasted_iota(jnp.int32, (1, LANES), 1)
+    wide = lax.broadcasted_iota(jnp.int32, (1, span), 1)
+    prev_t[...] = jnp.zeros_like(prev_t)
+
+    def prepare(j, slot):
+        arrived(0, slot)
+        arrived(1, slot)
+        d = dbuf[slot]
+        at = jnp.where(wide == len_ref[j] - 2, d, 0.0)
+        last = jnp.sum(at[:, :LANES] + at[:, LANES:], axis=1, keepdims=True)
+        dbuf[slot] = kbuf[slot].astype(F32) * jnp.exp(-d)
+        prev_t[...] = jnp.where(lane == j, last, prev_t[...])
+
+    def collect(i):
+        for copy in groups[i]:
+            copy.wait_recv()
+        copies.extend(groups[i])
+        _, _, place, width = parts[i]
+        cols = pl.ds(place, width)
+        total = part[me, :, cols]
+        for k in range(n - 1):
+            total = total + incoming[k, :, cols].astype(F32)
+        return total
+
+    def whole(which):
+        got = [collect(i) for i in range(len(parts)) if parts[i][0] == which]
+        return got[0] if len(got) == 1 else jnp.concatenate(got, axis=1)
+
+    @pl.loop(0, slots)
+    def _(j):
+        prepare(j, j)
+
     for copy in copies:
         copy.wait_recv()
-    total = part[me]
     square = sq_out[me]
     for k in range(n - 1):
-        total = total + incoming[k].astype(F32)
         square = square + sq_in[k]
-    sum_ref[...] = total
-    sq_ref[...] = square
-    for copy in copies:
+    scale = lax.rsqrt(square[:, :1] / D + NORM_EPS)
+    q = whole(0) * scale * KEY_WIDTH ** (-0.5)
+    pre = whole(4) * scale + bias_ref[...]
+    ld = (jnp.minimum(pre, 0.0) - jnp.log1p(jnp.exp(-jnp.abs(pre)))) / DECAY_SOFTNESS
+    spare = jnp.zeros((LANES - rows, keys), F32)
+    q_t[...] = jnp.concatenate([q, spare], axis=0).T
+    ld_t[...] = jnp.concatenate([ld, spare], axis=0).T
+
+    def weigh():
+        high, mid, low = split3(q_t[...] * jnp.exp(prev_t[...] + ld_t[...]))
+        a3[...] = (high + pltpu.roll(mid, rows, 1) + pltpu.roll(low, 2 * rows, 1)).astype(BF16)
+
+    ones = lax.broadcasted_iota(jnp.int32, (heads, 2 * sub), 1) % sub // 8
+    ones = (ones == lax.broadcasted_iota(jnp.int32, (heads, 2 * sub), 0)).astype(F32).astype(BF16)
+    own = lax.broadcasted_iota(jnp.int32, (heads, vals), 1) // DV
+    own = own == lax.broadcasted_iota(jnp.int32, (heads, vals), 0)
+    pick_row = lax.broadcasted_iota(jnp.int32, (LANES, 2 * LANES), 0)
+    pick_off = lax.broadcasted_iota(jnp.int32, (LANES, 2 * LANES), 1) // LANES
+
+    def fold(y):
+        return jnp.sum(y.reshape(heads, KEY_WIDTH // 8, 8, y.shape[1]), axis=1).reshape(sub, y.shape[1])
+
+    def spread(g):
+        pick = ((pick_row % rows == 2 * g + pick_off) & (pick_row < 3 * rows)).astype(F32)
+        ab[...] = jnp.dot(a3[...], pick.astype(BF16), preferred_element_type=F32)
+
+    def front(g, base):
+        for i in range(2):
+            j = 2 * g + i
+            slot = j - base
+            arrived(3, slot)
+            a = ab[:, i * LANES : (i + 1) * LANES]
+            z = jnp.concatenate(
+                [dbuf[slot, :, c : c + LANES] * a for c in range(0, span, LANES)], axis=1
+            )
+            s = jnp.dot(ones, stack2(fold(z)), preferred_element_type=F32)
+            score[i] = jnp.where(wide < len_ref[j] - 1, s, 0.0).astype(BF16)
+            c = fold(sbuf[slot].reshape(keys, DV) * a[:, :DV])
+            carry[i] = jnp.dot(ones, stack2(c), preferred_element_type=F32)
+
+    def back(g, base):
+        for i in range(2):
+            j = 2 * g + i
+            slot = j - base
+            arrived(2, slot)
+            got = lax.dot_general(score[i], vbuf[slot], NT, preferred_element_type=F32)
+            got = got + jnp.concatenate([carry[i]] * heads, axis=1)
+            raw[pl.ds(j, 1), :] = jnp.sum(jnp.where(own, got, 0.0), axis=0, keepdims=True)
+
+    def sweep(first, last, base, refill):
+        weigh()
+        spread(first)
+        front(first, base)
+        spread(jnp.minimum(first + 1, last - 1))
+
+        def refetch(g):
+            for i in range(2):
+                @pl.when(2 * g + i + slots < rows)
+                def _(i=i):
+                    fetch(2 * g + i + slots, 2 * g + i)
+
+        @pl.loop(first + 1, last)
+        def _(g):
+            back(g - 1, base)
+            front(g, base)
+            spread(jnp.minimum(g + 1, last - 1))
+            if refill:
+                refetch(g - 1)
+
+        back(last - 1, base)
+        if refill:
+            refetch(last - 1)
+
+    sweep(0, slots // 2, 0, slots < rows)
+    if slots < rows:
+        @pl.loop(slots, rows)
+        def _(j):
+            prepare(j, j - slots)
+
+        sweep(slots // 2, rows // 2, slots, False)
+
+    key_new = whole(1) * scale
+    v_new = whole(2) * scale
+    g = whole(3) * scale
+    qk = q * key_new
+    total = raw[...]
+    low = lane < DV
+    gain = jnp.concatenate([hg_ref[...]] * (LANES // DV), axis=1)
+    gate = g * (1.0 / (1.0 + jnp.exp(-g)))
+    for b in range(vals // LANES):
+        at = slice(b * LANES, (b + 1) * LANES)
+        both = []
+        for h in (2 * b, 2 * b + 1):
+            near = qk[:, h * KEY_WIDTH // LANES * LANES :][:, :LANES]
+            mine = lane // KEY_WIDTH == h * KEY_WIDTH % LANES // KEY_WIDTH
+            both.append(jnp.sum(jnp.where(mine, near, 0.0), axis=1, keepdims=True))
+        y = total[:, at] + jnp.where(low, both[0], both[1]) * v_new[:, at]
+        y2 = y * y
+        left = jnp.sum(jnp.where(low, y2, 0.0), axis=1, keepdims=True)
+        right = jnp.sum(jnp.where(low, 0.0, y2), axis=1, keepdims=True)
+        y = y * lax.rsqrt(jnp.where(low, left, right) / DV + NORM_EPS)
+        mixed[:, at] = (y * gain * gate[:, at]).astype(BF16)
+    group = [
+        send("kv", k, lambda p: mixed, gath.at[me], g_s.at[k - 1], g_r.at[k - 1])
+        for k in SEND_ORDER(n)
+    ]
+    out_ref[me] = mixed[...]
+    for copy in group:
+        copy.wait_recv()
+    for k in range(1, n):
+        peer = lax.rem(me + k, n)
+        out_ref[peer] = gath[peer]
+    for copy in copies + group:
         copy.wait_send()
 
 
-def SEND_ORDER(n):
-    return sorted(range(1, n), key=lambda k: -min(k, n - k))
-
-
-def project(tokens, gain, weights):
+def attend(
+    tokens, gain, weights, span_lengths, bias, head_gain, keys, values, decays, state
+):
     n = lax.axis_size("kv")
-    rows = tokens.shape[0] // n
+    rows, heads = state.shape[:2]
+    kw, vw, span = heads * KEY_WIDTH, heads * DV, keys.shape[2]
+    slots = min(rows, 24)
     parts, place = [], 0
-    for which, w in enumerate(weights):
+    for which in (0, 4, 1, 2, 3):
+        w = weights[which]
         width = min(512, w.shape[1])
         for col in range(0, w.shape[1], width):
             parts.append((which, col, place, width))
             place += width
     vmem = pl.BlockSpec(memory_space=pltpu.VMEM)
+    hbm = pl.BlockSpec(memory_space=pltpu.HBM)
+    dma = pltpu.SemaphoreType.DMA
     return pl.pallas_call(
-        functools.partial(project_kernel, parts),
-        out_shape=(
-            jax.ShapeDtypeStruct((rows, place), F32),
-            jax.ShapeDtypeStruct((rows, LANES), F32),
-        ),
-        in_specs=[vmem, vmem] + [pl.BlockSpec(memory_space=pltpu.HBM)] * 5,
-        out_specs=(vmem, vmem),
+        functools.partial(attend_kernel, parts, slots),
+        out_shape=jax.ShapeDtypeStruct((n, rows, vw), BF16),
+        in_specs=[pl.BlockSpec(memory_space=pltpu.SMEM)] + [vmem] * 4 + [hbm] * 9,
+        out_specs=vmem,
         scratch_shapes=[
             pltpu.VMEM((tokens.shape[1], place), BF16),
             pltpu.VMEM((n, rows, place), F32),
@@ -133,170 +313,44 @@
             pltpu.VMEM((n - 1, rows, place), BF16),
             pltpu.VMEM((n, rows, LANES), F32),
             pltpu.VMEM((n - 1, rows, LANES), F32),
-            pltpu.SemaphoreType.DMA((len(parts),)),
-            pltpu.SemaphoreType.DMA((n - 1, len(parts))),
-            pltpu.SemaphoreType.DMA((n - 1, len(parts))),
-            pltpu.SemaphoreType.DMA((n - 1,)),
-            pltpu.SemaphoreType.DMA((n - 1,)),
+            pltpu.VMEM((slots, kw, span), BF16),
+            pltpu.VMEM((slots, vw, span), BF16),
+            pltpu.VMEM((slots, kw, span), F32),
+            pltpu.VMEM((slots, heads, KEY_WIDTH, DV), F32),
+            pltpu.VMEM((kw, LANES), F32),
+            pltpu.VMEM((kw, LANES), F32),
+            pltpu.VMEM((kw, LANES), F32),
+            pltpu.VMEM((kw, LANES), BF16),
+            pltpu.VMEM((kw, 2 * LANES), F32),
+            pltpu.VMEM((2, heads, span), BF16),
+            pltpu.VMEM((2, heads, DV), F32),
+            pltpu.VMEM((rows, vw), F32),
+            pltpu.VMEM((rows, vw), BF16),
+            pltpu.VMEM((n, rows, vw), BF16),
+            dma((len(parts),)),
+            dma((4, slots)),
+            dma((n - 1, len(parts))),
+            dma((n - 1, len(parts))),
+            dma((n - 1,)),
+            dma((n - 1,)),
+            dma((n - 1,)),
+            dma((n - 1,)),
         ],
         compiler_params=pltpu.CompilerParams(
-            collective_id=0, has_side_effects=True, vmem_limit_bytes=62 << 20
-        ),
-        name="project",
-    )(tokens, gain.reshape(1, -1), *weights)
-
-
-NT = (((1,), (1,)), ((), ()))
-
-
-def attend_kernel(
-    len_ref, last_ref, sum_ref, sq_ref, bias_ref, hg_ref, k1, k2a, k2b, d1, d2a, d2b,
-    v1, v2a, v2b, st, out_ref, q_t, ld_t, qk_t, vn, gs, now_s, q_s, hist, raw,
-):
-    step = pl.program_id(0)
-    rows = out_ref.shape[0]
-    heads = st.shape[1]
-    keys, vals = heads * KEY_WIDTH, heads * DV
-    lane = lax.broadcasted_iota(jnp.int32, (1, LANES), 1)
-
-    @pl.when(step == 0)
-    def _():
-        scale = lax.rsqrt(sq_ref[:, :1] / D + NORM_EPS)
-        q = sum_ref[:, :keys] * scale * KEY_WIDTH ** (-0.5)
-        key_new = sum_ref[:, keys : 2 * keys] * scale
-        at = 2 * keys
-        vn[...] = sum_ref[:, at : at + vals] * scale
-        g = sum_ref[:, at + vals : at + 2 * vals] * scale
-        gs[...] = g * (1.0 / (1.0 + jnp.exp(-g))) * jnp.concatenate([hg_ref[...]] * heads, axis=1)
-        x = sum_ref[:, at + 2 * vals :] * scale + bias_ref[...]
-        ld = (jnp.minimum(x, 0.0) - jnp.log1p(jnp.exp(-jnp.abs(x)))) / DECAY_SOFTNESS
-        spare = jnp.zeros((LANES - rows, keys), F32)
-        q_t[...] = jnp.concatenate([q, spare], axis=0).T
-        ld_t[...] = jnp.concatenate([ld, spare], axis=0).T
-        pick = lax.broadcasted_iota(jnp.int32, (heads, keys), 1) // KEY_WIDTH
-        pick = (pick == lax.broadcasted_iota(jnp.int32, (heads, keys), 0)).astype(F32)
-        qk_t[...] = lax.dot_general(
-            pick,
-            jnp.concatenate([q * key_new, spare], axis=0),
-            NT,
-            precision=lax.Precision.HIGHEST,
-            preferred_element_type=F32,
-        )
-
-    seconds = ((k2a, d2a, v2a), (k2b, d2b, v2b))
-    lengths = [len_ref[2 * step + j] for j in range(2)]
-    mine = [lane == 2 * step + j for j in range(2)]
-    wide = (keys, LANES)
-
-    def block(j, k, d, v, offset):
-        s = k.astype(F32) * q_s[j] * jnp.exp(now_s[j] - d)
-        s = jnp.sum(s.reshape(heads, KEY_WIDTH, LANES), axis=1)
-        s = jnp.where(lane + offset < lengths[j] - 1, s, 0.0).astype(BF16)
-        return lax.dot_general(s, v, NT, preferred_element_type=F32)
-
-    for j in range(2):
-        prev = jnp.where(lane == lengths[j] - 2, d1[j], 0.0)
-        prev = prev + jnp.where(lane + LANES == lengths[j] - 2, seconds[j][1][0], 0.0)
-        own_decay = jnp.where(mine[j], ld_t[...], 0.0)
-        now_s[j] = jnp.broadcast_to(jnp.sum(prev + own_decay, axis=1, keepdims=True), wide)
-        q = jnp.sum(jnp.where(mine[j], q_t[...], 0.0), axis=1, keepdims=True)
-        q_s[j] = jnp.broadcast_to(q, wide)
-    for j in range(2):
-        hist[j] = block(j, k1[j], d1[j], v1[j], 0)
-    for j in range(2):
-
-        @pl.when(lengths[j] - 1 > LANES)
-        def _(j=j):
-            k2, d2, v2 = seconds[j]
-            hist[j] += block(j, k2[0], d2[0], v2[0], LANES)
-
-    own = lax.broadcasted_iota(jnp.int32, (heads, vals), 1) // DV
-    own = own == lax.broadcasted_iota(jnp.int32, (heads, vals), 0)
-    for j in range(2):
-        weight = (q_s[j] * jnp.exp(now_s[j]))[:, :DV]
-        carried = weight * st[j].reshape(keys, DV)
-        carried = jnp.sum(carried.reshape(heads, KEY_WIDTH, DV), axis=1)
-        carried = jnp.concatenate([carried] * heads, axis=1)
-        qk = jnp.sum(jnp.where(mine[j], qk_t[...], 0.0), axis=1, keepdims=True)
-        row = pl.ds(2 * step + j, 1)
-        whole = hist[j] + carried + qk * vn[row, :]
-        whole = jnp.where(own, whole, 0.0)
-        mean = jnp.sum(whole * whole, axis=1, keepdims=True) / DV
-        whole = whole * lax.rsqrt(mean + NORM_EPS)
-        raw[row, :] = jnp.sum(whole, axis=0, keepdims=True)
-
-    @pl.when(step == pl.num_programs(0) - 1)
-    def _():
-        out_ref[...] = (raw[...] * gs[...]).astype(BF16)
-
-
-def attend(span_lengths, sums, square, bias, head_gain, keys, values, decays, state):
-    rows, heads = state.shape[:2]
-    kw, vw = heads * KEY_WIDTH, heads * DV
-    order = jnp.arange(rows, dtype=jnp.int32)
-    needed = jnp.where(span_lengths - 1 > LANES, order, order % 2)
-    before = (order[None, :] <= order[:, None]) & (order[None, :] % 2 == order[:, None] % 2)
-    last = jnp.max(jnp.where(before, needed[None, :], 0), axis=1)
-
-    def first(width):
-        return pl.BlockSpec((2, width, LANES), lambda i, ln, la: (i, 0, 0))
-
-    def second(width, j):
-        return pl.BlockSpec((1, width, LANES), lambda i, ln, la: (la[2 * i + j], 0, 1))
-
-    def fixed(shape):
-        return pl.BlockSpec(shape, lambda i, ln, la: (0,) * len(shape))
-
-    return pl.pallas_call(
-        attend_kernel,
-        out_shape=jax.ShapeDtypeStruct((rows, vw), BF16),
-        grid_spec=pltpu.PrefetchScalarGridSpec(
-            num_scalar_prefetch=2,
-            grid=(rows // 2,),
-            in_specs=[
-                fixed(sums.shape),
-                fixed(square.shape),
-                fixed((1, kw)),
-                fixed((1, DV)),
-                first(kw),
-                second(kw, 0),
-                second(kw, 1),
-                first(kw),
-                second(kw, 0),
-                second(kw, 1),
-                first(vw),
-                second(vw, 0),
-                second(vw, 1),
-                pl.BlockSpec((2, heads, KEY_WIDTH, DV), lambda i, ln, la: (i, 0, 0, 0)),
-            ],
-            out_specs=fixed((rows, vw)),
-            scratch_shapes=[
-                pltpu.VMEM((kw, LANES), F32),
-                pltpu.VMEM((kw, LANES), F32),
-                pltpu.VMEM((heads, LANES), F32),
-                pltpu.VMEM((rows, vw), F32),
-                pltpu.VMEM((rows, vw), F32),
-                pltpu.VMEM((2, kw, LANES), F32),
-                pltpu.VMEM((2, kw, LANES), F32),
-                pltpu.VMEM((2, heads, vw), F32),
-                pltpu.VMEM((rows, vw), F32),
-            ],
-        ),
-        compiler_params=pltpu.CompilerParams(
-            dimension_semantics=("arbitrary",), vmem_limit_bytes=62 << 20
+            collective_id=0, has_side_effects=True, vmem_limit_bytes=63 << 20
         ),
         name="attend",
     )(
-        span_lengths, last, sums, square, bias.reshape(1, -1), head_gain.reshape(1, -1),
-        keys, keys, keys, decays, decays, decays, values, values, values, state,
+        span_lengths, tokens, gain.reshape(1, -1), bias.reshape(1, -1),
+        head_gain.reshape(1, -1), *weights, keys, values, decays, state,
     )
 
 
 def finish_kernel(
     mixed_ref, tok_ref, gain_ref, ow_ref, uw_ref, dw_ref, out_ref,
-    ow, uw, dw, gath, part, t_out, t_in, resid, scaled, sq_out, sq_in,
+    ow, uw, dw, part, t_out, t_in, resid, scaled, sq_out, sq_in,
     u_part, u_own, u_out, u_in, hid, total, t_out2, t_in2, done,
-    wsem, g_s, g_r, a_s, a_r, b_s, b_r, q_s, q_r, u_s, u_r, h_s, h_r, c_s, c_r, e_s, e_r,
+    wsem, a_s, a_r, b_s, b_r, q_s, q_r, u_s, u_r, h_s, h_r, c_s, c_r, e_s, e_r,
 ):
     n, m = lax.axis_size("kv"), lax.axis_size("tp")
     me, col = lax.axis_index("kv"), lax.axis_index("tp")
@@ -319,14 +373,8 @@
             copy.wait_recv()
         copies.extend(group)
 
-    group = [
-        send("kv", k, lambda p: mixed_ref, gath.at[me], g_s.at[k - 1], g_r.at[k - 1])
-        for k in SEND_ORDER(n)
-    ]
-    gath[me] = mixed_ref[...]
-    wait_all(group)
     loads[0].wait()
-    rows = gath.shape[0] * gath.shape[1]
+    rows = mixed_ref.shape[0] * mixed_ref.shape[1]
 
     def over_tp(value, outgoing, incoming, ss, rs):
         part[...] = value.reshape(part.shape)
@@ -348,7 +396,7 @@
         ]
         wait_all(group)
 
-    x = gath[...].reshape(rows, gath.shape[2])
+    x = mixed_ref[...].reshape(rows, mixed_ref.shape[2])
     attn = over_tp(jnp.dot(x, ow[...], preferred_element_type=F32), t_out, t_in, a_s, a_r)
     resid[col] = (tok_ref[col].astype(F32) + attn).astype(BF16)
     to_tp(resid, b_s, b_r)
@@ -436,7 +484,7 @@
 def finish(mixed, tokens, gain, out_weight, up_weight, down_weight):
     n, m = lax.axis_size("kv"), lax.axis_size("tp")
     rows, feats = tokens.shape
-    vals, hidden = out_weight.shape[0], up_weight.shape[1]
+    hidden = up_weight.shape[1]
     own, share = rows // n, rows // m
     chunks = 4
     vmem = pl.BlockSpec(memory_space=pltpu.VMEM)
@@ -451,7 +499,6 @@
             pltpu.VMEM(out_weight.shape, BF16),
             pltpu.VMEM(up_weight.shape, BF16),
             pltpu.VMEM(down_weight.shape, BF16),
-            pltpu.VMEM((n, own, vals), BF16),
             pltpu.VMEM((m, share, feats), F32),
             pltpu.VMEM((m, share, feats), BF16),
             pltpu.VMEM((m - 1, share, feats), BF16),
@@ -469,8 +516,6 @@
             pltpu.VMEM((m - 1, share, feats), BF16),
             pltpu.VMEM((m, share, feats), BF16),
             dma((2 + chunks,)),
-            dma((n - 1,)),
-            dma((n - 1,)),
             dma((m - 1,)),
             dma((m - 1,)),
             dma((m - 1,)),
@@ -518,9 +563,8 @@
     down_weight,
 ):
     weights = (query_weight, key_weight, value_weight, gate_weight, decay_matrix)
-    sums, square = project(tokens, attn_gain, weights)
     mixed = attend(
-        span_lengths, sums, square, decay_offset_bias, head_gain,
+        tokens, attn_gain, weights, span_lengths, decay_offset_bias, head_gain,
         key_cache, value_cache, decay_cache, block_state,
     )
     return finish(mixed, tokens, mixer_gain, out_weight, up_weight, down_weight)
@@ -534,7 +578,9 @@
         and rows % 16 == 0
         and share % 16 == 0
         and heads % 8 == 0
-        and rows < LANES
+        and 3 * rows <= LANES
+        and rows % 4 == 0
+        and DV * 2 == LANES
         and key_cache.shape[2] == 2 * LANES
     )
 

time: 131 us -> 114 us (0.87); the launches traced: 129 us -> 114 us
  Pallas kernels: 126 us -> 113 us
  other arithmetic: 1.43 us -> 0 us
    pallas_call x2 -> x1, Pallas kernels: 53 us -> 44.8 us  [attend(): pl.pallas_call(functools.partial(attend_kernel, parts, slots), out_shape=...]
    pallas_call x1, Pallas kernels: 73.2 us -> 67.7 us  [finish(): pl.pallas_call(finish_kernel, out_shape=jax.ShapeDtypeStruct((m, share, f...]
where the time goes in v1:
time: 114 us
  Pallas kernels  113 us (99%)
  local copies, waits for them, and re-layouts  1.67 us (1%)
    pallas_call x1, Pallas kernels, finish(): pl.pallas_call(finish_kernel, out_shape=jax.ShapeDtypeStruct((m, share, f...  67.7 us
    pallas_call x1, Pallas kernels, attend(): pl.pallas_call(functools.partial(attend_kernel, parts, slots), out_shape=...  44.8 us

profile of v1, /device:TPU:1, one launch (start us, length us, event | category | flops | bytes accessed | tf_op | source)
XLA Modules:
  0.0 114.2 jit_solution(16381273198602055638)
XLA Ops:
  0.0 44.8 %attend.1.mixed_ref = bf16[4,32,1024]{2,1,0:T(8,128)(2,1)} custom-call(s32[32]{0:T(128)} %len_ref.1, bf16[128,1024]{1,0:T(8,128)(2,1)} %tok_ref.1, f32[1,1024]{1,0:T(1,128)} %bitcast.8, f32[1,512]{1,0:T(1,128)} %bitcast.10, f32[1,64]{1,0:T(1,128)} %bitcast.11, bf16[1024,512]{1,0:T(8,128)(2,1)} %refs_0_.1, bf16[1024,512]{1,0:T(8,128)(2,1)} %refs_1_.1, ...), custom_call_target="tpu_custom_call" | custom-call | tf_op jit(solution)/shard_map/attend/pallas_call | solution.py:304
  44.8 67.7 %finish.1 = bf16[4,32,1024]{2,1,0:T(8,128)(2,1)} custom-call(bf16[4,32,1024]{2,1,0:T(8,128)(2,1)} %attend.1.mixed_ref, bf16[4,32,1024]{2,1,0:T(8,128)(2,1)} %bitcast.6, f32[1,1024]{1,0:T(1,128)} %bitcast.9, bf16[1024,1024]{1,0:T(8,128)(2,1)} %ow_ref.1, bf16[1024,4096]{1,0:T(8,128)(2,1)} %uw_ref.1, bf16[4096,1024]{1,0:T(8,128)(2,1)} %dw_ref.1), custom_call_target="tpu_custom_call" | custom-call | tf_op jit(solution)/shard_map/finish/pallas_call | solution.py:493
  112.5 1.7 %copy.20 = bf16[128,1024]{1,0:T(8,128)(2,1)} copy(bf16[128,1024]{1,0:T(8,128)(2,1)} %bitcast.7) | data formatting | bytes 524288
